TPU v7x, 32 devices: a whole 2x2x4 slice. The times are simulated.
32 devices in a mesh: fs: 8 (over z, y), tp: 4 (over x, core).
Axes of the slice: x: 2, y: 2, z: 4, core: 2. Of those that a mesh axis runs over, the one named last changes fastest.
Arguments:
- inputs: bfloat16 [4608, 2048], P('fs'), may hold values from -6 to 6
- query_cotangent: bfloat16 [4608, 1024], P('fs', 'tp'), may hold values from -0.017944336 to 0.017944336
- value_cotangent: bfloat16 [4608, 1024], P('fs', 'tp'), may hold values from -0.017944336 to 0.017944336
- weights_query: float32 [2048, 1024], P('fs', 'tp'), may hold values from -6 to 6
- weights_value: float32 [2048, 1024], P('fs', 'tp'), may hold values from -6 to 6
- basis_query: bfloat16 [1024, 32], P('tp'), may hold values from -0.75 to 0.75
- basis_value: bfloat16 [1024, 32], P('tp'), may hold values from -0.75 to 0.75
- first_query: float32 [2048, 512], P('fs', 'tp'), may hold values from -5.4 to 5.4, as said below
- second_query: float32 [2048, 512], P('fs', 'tp'), may hold values from 0.05 to 1
- first_value: float32 [2048, 512], P('fs', 'tp'), may hold values from -5.4 to 5.4, as said below
- second_value: float32 [2048, 512], P('fs', 'tp'), may hold values from 0.05 to 1
Outputs:
- step_query: float32 [2048, 1024], P('fs', 'tp')
- step_value: float32 [2048, 1024], P('fs', 'tp')
- new_query: float32 [2048, 1024], P('fs', 'tp')
- new_value: float32 [2048, 1024], P('fs', 'tp')
- copy_query: bfloat16 [2048, 1024], P(None, 'tp')
- copy_value: bfloat16 [2048, 1024], P(None, 'tp')
- moment_query: float32 [2048, 512], P('fs', 'tp')
- square_query: float32 [2048, 512], P('fs', 'tp')
- moment_value: float32 [2048, 512], P('fs', 'tp')
- square_value: float32 [2048, 512], P('fs', 'tp')
Inputs may be any that keep to these rules, and one draw needn't show every extreme that they name: `first_query`: first moments, with a spread of scale from row to row. `first_value`: first moments, with a spread of scale from row to row.
All inputs are finite; a program needn't handle non-finite values.
Results may differ from a plain program's by a relative error of at most 0.003.
Values may be sent and summed in bfloat16 or wider, within the bound.
A program may use at most 64 MiB of HBM per device.

v0:
```python
import jax
import jax.numpy as jnp
from jax import lax
from jax.sharding import PartitionSpec as P

D = 2048
HEADS = 16
HEAD = 64
RK = 32


def from_space(direction, factor, heads_here):
    count = direction.shape[0]
    split = direction.reshape(count, heads_here, RK)
    out = jnp.einsum("nhr,hdr->nhd", split, factor, precision=lax.Precision.HIGHEST)
    return out.reshape(count, heads_here * HEAD)


def moments(reduced, first, second):
    moment = 0.9 * first + 0.1 * reduced
    square = 0.95 * second + 0.05 * reduced * reduced
    direction = moment / (jnp.sqrt(square) + 1e-08)
    return (moment, square, direction)


def per_device(
    inputs,
    query_cotangent,
    value_cotangent,
    weights_query,
    weights_value,
    basis_query,
    basis_value,
    first_query,
    second_query,
    first_value,
    second_value,
):
    own_cols = weights_query.shape[1]
    heads_here = own_cols // HEAD
    space_cols = heads_here * RK
    factor_q = basis_query.reshape(heads_here, HEAD, RK).astype(jnp.float32)
    factor_v = basis_value.reshape(heads_here, HEAD, RK).astype(jnp.float32)
    contract = (((0,), (0,)), ((), ()))
    tok_count = query_cotangent.shape[0]
    bf_q = basis_query.reshape(heads_here, HEAD, RK)
    bf_v = basis_value.reshape(heads_here, HEAD, RK)
    small_q = jnp.einsum(
        "thd,hdr->thr",
        query_cotangent.reshape(tok_count, heads_here, HEAD),
        bf_q,
        preferred_element_type=jnp.float32,
    )
    small_v = jnp.einsum(
        "thd,hdr->thr",
        value_cotangent.reshape(tok_count, heads_here, HEAD),
        bf_v,
        preferred_element_type=jnp.float32,
    )
    small_both = jnp.concatenate(
        (small_q.reshape(tok_count, space_cols), small_v.reshape(tok_count, space_cols)), axis=1
    )
    upper_part = small_both.astype(jnp.bfloat16)
    lower_part = (small_both - upper_part.astype(jnp.float32)).astype(jnp.bfloat16)
    high = lax.dot_general(inputs, upper_part, contract, preferred_element_type=jnp.float32)
    reduced = lax.psum_scatter(
        high + lax.dot_general(inputs, lower_part, contract, preferred_element_type=jnp.float32),
        "fs",
        scatter_dimension=0,
        tiled=True,
    )
    reduced_q = reduced[:, :space_cols]
    reduced_v = reduced[:, space_cols:]
    moment_q, square_q, direction_q = moments(reduced_q, first_query, second_query)
    moment_v, square_v, direction_v = moments(reduced_v, first_value, second_value)
    total_q, total_v = lax.psum(
        (jnp.sum(direction_q * direction_q), jnp.sum(direction_v * direction_v)), ("fs", "tp")
    )
    entries = D * HEADS * RK
    scale_q = 1.0 / jnp.sqrt(total_q / entries + 0.25)
    scale_v = 1.0 / jnp.sqrt(total_v / entries + 0.25)
    step_q = scale_q * from_space(direction_q, factor_q, heads_here)
    step_v = scale_v * from_space(direction_v, factor_v, heads_here)
    fresh_q = weights_query - 0.1 * step_q
    fresh_v = weights_value - 0.1 * step_v
    copy_q, copy_v = (
        lax.all_gather(fresh_q.astype(jnp.bfloat16), "fs", axis=0, tiled=True),
        lax.all_gather(fresh_v.astype(jnp.bfloat16), "fs", axis=0, tiled=True),
    )
    return (
        step_q,
        step_v,
        fresh_q,
        fresh_v,
        copy_q,
        copy_v,
        moment_q,
        square_q,
        moment_v,
        square_v,
    )


def solution(mesh):
    placed = (
        P("fs", None),
        P("fs", "tp"),
        P("fs", "tp"),
        P("fs", "tp"),
        P("fs", "tp"),
        P("tp", None),
        P("tp", None),
        P("fs", "tp"),
        P("fs", "tp"),
        P("fs", "tp"),
        P("fs", "tp"),
    )
    return jax.shard_map(
        per_device,
        mesh=mesh,
        in_specs=placed,
        out_specs=(
            P("fs", "tp"),
            P("fs", "tp"),
            P("fs", "tp"),
            P("fs", "tp"),
            P(None, "tp"),
            P(None, "tp"),
            P("fs", "tp"),
            P("fs", "tp"),
            P("fs", "tp"),
            P("fs", "tp"),
        ),
        check_vma=False,
    )
```

profile of v0, /device:TPU:0, one launch (start us, length us, event | category | flops | bytes accessed | tf_op | source)
XLA Modules:
  0.0 223.8 jit_solution(16746739006652718097)
XLA Ops:
  7.2 0.0 copy-start
  7.2 0.0 reduce-scatter.2.cloned.1.call-start
  7.2 1.0 reshape.52
  8.2 0.0 copy-start.4
  8.2 0.8 reshape.55
  9.0 1.2 copy.40
  10.2 1.2 copy.42
  11.4 0.2 fusion.10
  11.6 0.2 fusion.7
  11.7 0.0 copy-done
  11.8 1.0 fusion.2
  12.8 0.0 copy-done.4
  12.8 0.0 copy-start.5
  12.8 2.3 %fusion = f32[2048,256]{0,1:T(8,128)} fusion(f32[256,2048]{1,0:T(8,128)S(1)} %fusion.2, bf16[576,2048]{1,0:T(8,128)(2,1)S(1)} %copy-done, f32[576,128]{0,1:T(8,128)S(1)} %bitcast.31, f32[576,128]{0,1:T(8,128)S(1)} %bitcast.29), kind=kOutput, calls=%fused_computation.1 | convolution fusion | flops 605241344 | bytes 7143424 | tf_op jit(solution)/shard_map/dot_general | solution.py:67
  15.1 0.0 copy-start.6
  15.1 0.0 copy-start.7
  15.1 0.0 copy-start.8
  15.1 0.0 reduce-scatter.2.cloned.1.call-update
  15.2 0.0 all-gather.5.cloned.1.call-start
  15.2 0.0 copy-done.5
  15.2 0.1 copy.39
  15.3 0.7 copy-done.6
  16.0 0.1 copy.44
  16.1 0.0 copy-done.7
  16.1 0.1 copy.46
  16.3 0.0 copy-done.8
  16.3 0.1 copy.47
  16.4 70.6 %reduce-scatter.2.cloned.1.call-done = f32[256,256]{0,1:T(8,128)} async-done(((f32[2048,256]{0,1:T(8,128)}), f32[256,256]{0,1:T(8,128)}) %reduce-scatter.2.cloned.1.call-update) | async-done | bytes 262160 | tf_op jit(solution)/shard_map/reduce_scatter | solution.py:66
  86.9 2.4 %multiply_reduce_fusion = (f32[]{:T(128)}, f32[256,128]{0,1:T(8,128)S(1)}, f32[256,128]{0,1:T(8,128)}, f32[256,128]{0,1:T(8,128)S(1)}, f32[]{:T(128)}, /*index=5...) fusion(f32[256,256]{0,1:T(8,128)} %reduce-scatter.2.cloned.1.call-done, f32[256,128]{0,1:T(8,128)S(1)} %copy.47, ...), kind=kLoop, calls=%fused_computation.14 | loop fusion | flops 720894 | bytes 1572872 | tf_op jit(solution)/shard_map/reduce_sum | solution.py:77
  89.3 39.8 %all-reduce = (f32[]{:T(128)}, f32[]{:T(128)}) all-reduce(f32[]{:T(128)} %get-tuple-element.44, f32[]{:T(128)} %get-tuple-element.36), channel_id=1, replica_groups=mesh['fs'=8,'tp'=4] {'fs','tp'}, use_global_device_ids=true, to_apply=%region_2.0 | all-reduce | flops 2 | bytes 16 | tf_op jit(solution)/shard_map/psum | solution.py:76
  129.8 0.3 convolution_multiply_fusion
  130.1 0.1 copy.52
  130.3 0.0 copy-start.1
  130.3 1.8 fusion.14
  132.1 0.0 all-gather.5.cloned.1.call-update
  132.1 0.0 all-gather.3.cloned.1.call-start
  132.9 1.2 convolution_multiply_fusion.1
  134.1 0.1 copy.51
  134.2 0.0 copy-start.2
  134.2 1.8 fusion.15
  136.1 0.0 all-gather.3.cloned.1.call-update
  136.1 1.7 copy.56
  137.8 0.8 copy.55
  138.5 0.8 copy.54
  139.3 0.8 copy.53
  140.0 32.2 %all-gather.5.cloned.1.call-done = bf16[2048,256]{1,0:T(8,128)(2,1)} async-done(((bf16[256,256]{1,0:T(8,128)(2,1)}), bf16[2048,256]{1,0:T(8,128)(2,1)}) %all-gather.5.cloned.1.call-update) | async-done | bytes 1048592 | tf_op jit(solution)/shard_map/all_gather | solution.py:88
  172.3 41.7 %all-gather.3.cloned.1.call-done = bf16[2048,256]{1,0:T(8,128)(2,1)} async-done(((bf16[256,256]{1,0:T(8,128)(2,1)}), bf16[2048,256]{1,0:T(8,128)(2,1)}) %all-gather.3.cloned.1.call-update) | async-done | bytes 1048592 | tf_op jit(solution)/shard_map/all_gather | solution.py:87
  214.0 0.0 copy-start.3
  214.0 2.4 %copy.67 = bf16[2048,256]{1,0:T(8,128)(2,1)} copy(bf16[2048,256]{1,0:T(8,128)(2,1)} %all-gather.3.cloned.1.call-done) | data formatting | bytes 2097152
  216.3 0.0 copy-done.1
  216.3 0.0 copy-done.3
  216.3 1.0 copy.68
  217.3 0.0 copy-done.2
Async XLA Ops:
  7.2 4.6 %copy-start = (bf16[576,2048]{1,0:T(8,128)(2,1)S(1)}, bf16[576,2048]{1,0:T(8,128)(2,1)}, u32[]{:S(2)}) copy-start(bf16[576,2048]{1,0:T(8,128)(2,1)} %param.11) | copy-start | bytes 7077892
  7.2 79.7 %reduce-scatter.2.cloned.1.call-start = ((), (), s32[]{:S(2)}) async-start(), calls=%async_computation.1 | async-start | bytes 2359296 | tf_op jit(solution)/shard_map/reduce_scatter | solution.py:66
  8.2 4.6 %copy-start.4 = (bf16[4,64,32]{1,0,2:T(4,128)(2,1)}, bf16[4,64,32]{1,0,2:T(4,128)(2,1)S(1)}, u32[]{:S(2)}) copy-start(bf16[4,64,32]{1,0,2:T(4,128)(2,1)S(1)} %reshape.52) | copy-start | bytes 49156
  12.8 2.4 %copy-start.5 = (f32[256,128]{1,0:T(8,128)S(1)}, f32[256,128]{1,0:T(8,128)}, u32[]{:S(2)}) copy-start(f32[256,128]{1,0:T(8,128)} %param.18) | copy-start | bytes 393220
  15.1 0.9 copy-start.6
  15.1 1.0 copy-start.7
  15.1 1.1 copy-start.8
  15.2 157.1 %all-gather.5.cloned.1.call-start = ((), (), s32[]{:S(2)}) async-start(), calls=%async_computation.3 | async-start | bytes 1179648 | tf_op jit(solution)/shard_map/all_gather | solution.py:88
  130.3 86.1 %copy-start.1 = (f32[256,256]{1,0:T(8,128)}, f32[256,256]{1,0:T(8,128)S(1)}, u32[]{:S(2)}) copy-start(f32[256,256]{1,0:T(8,128)S(1)} %copy.52) | copy-start | bytes 786436
  132.1 81.8 %all-gather.3.cloned.1.call-start = ((), (), s32[]{:S(2)}) async-start(), calls=%async_computation.2 | async-start | bytes 1179648 | tf_op jit(solution)/shard_map/all_gather | solution.py:87
  134.2 83.1 %copy-start.2 = (f32[256,256]{1,0:T(8,128)}, f32[256,256]{1,0:T(8,128)S(1)}, u32[]{:S(2)}) copy-start(f32[256,256]{1,0:T(8,128)S(1)} %copy.51) | copy-start | bytes 786436
  214.0 2.4 %copy-start.3 = (bf16[2048,256]{1,0:T(8,128)(2,1)S(1)}, bf16[2048,256]{1,0:T(8,128)(2,1)}, u32[]{:S(2)}) copy-start(bf16[2048,256]{1,0:T(8,128)(2,1)} %all-gather.5.cloned.1.call-done) | copy-start | bytes 3145732
Sparse Core Ops, SparseCore 0:
  15.3 71.6 reduce-scatter.1
  132.3 39.9 all-gather.4
  175.0 38.9 all-gather.2
where the time goes:
time: 224 us
  waiting for transfers between devices  145 us (65%)
  blocking collectives  39.8 us (18%)
  between operations  15.3 us (7%)
  local copies, waits for them, and re-layouts  12.7 us (6%)
  other arithmetic  6.06 us (3%)
  matrix products  5.25 us (2%)
    reduce_scatter x1, waiting for transfers between devices, per_device(): lax.psum_scatter(high + lax.dot_general(inputs, lower_part, contract, pre...  70.6 us
    all_gather x1, waiting for transfers between devices, per_device(): lax.all_gather(fresh_q.astype(jnp.bfloat16), 'fs', axis=0, tiled=True)  41.7 us
    psum x1, blocking collectives, per_device(): lax.psum((jnp.sum(direction_q * direction_q), jnp.sum(direction_v * direc...  39.8 us
    all_gather x1, waiting for transfers between devices, per_device(): lax.all_gather(fresh_v.astype(jnp.bfloat16), 'fs', axis=0, tiled=True)  32.2 us
    unnamed x32, local copies, waits for them, and re-layouts  11 us
  transfers between devices with their start and end apart: 3, of which 3 were waited for; matrix products, arithmetic and copies ran while one was open for 3% of the time, Pallas kernels for 0%

commit v1 on v0

--- a/solution.py
+++ b/solution.py
@@ -7,6 +7,22 @@
 HEADS = 16
 HEAD = 64
 RK = 32
+
+
+def collect(x, axis, dim):
+    ways, here, turn = (lax.axis_size(axis), lax.axis_index(axis), x.shape[dim])
+    lengths = [n * ways if d == dim else n for d, n in enumerate(x.shape)]
+    full = lax.dynamic_update_slice_in_dim(jnp.zeros(lengths, x.dtype), x, here * turn, axis=dim)
+    going_up = going_down = x
+    for far in range(1, ways // 2 + 1):
+        going_up = lax.ppermute(going_up, axis, [(d, (d + 1) % ways) for d in range(ways)])
+        full = lax.dynamic_update_slice_in_dim(full, going_up, (here - far) % ways * turn, axis=dim)
+        if 2 * far < ways:
+            going_down = lax.ppermute(going_down, axis, [(d, (d - 1) % ways) for d in range(ways)])
+            full = lax.dynamic_update_slice_in_dim(
+                full, going_down, (here + far) % ways * turn, axis=dim
+            )
+    return full
 
 
 def from_space(direction, factor, heads_here):
@@ -84,7 +100,7 @@
     fresh_q = weights_query - 0.1 * step_q
     fresh_v = weights_value - 0.1 * step_v
     copy_q, copy_v = (
-        lax.all_gather(fresh_q.astype(jnp.bfloat16), "fs", axis=0, tiled=True),
+        collect(fresh_q.astype(jnp.bfloat16), "fs", 0),
         lax.all_gather(fresh_v.astype(jnp.bfloat16), "fs", axis=0, tiled=True),
     )
     return (

time: 224 us -> 188 us (0.84)
  waiting for transfers between devices: 145 us -> 88.2 us
  starting transfers between devices: 0.12 us -> 14.2 us
  local copies, waits for them, and re-layouts: 12.7 us -> 17.4 us
    all_gather x1 -> x0, waiting for transfers between devices: 41.7 us -> none  [per_device(): lax.all_gather(fresh_q.astype(jnp.bfloat16), 'fs', axis=0, tiled=True)]
    all_gather x1, waiting for transfers between devices: 32.2 us -> 5.64 us  [per_device(): lax.all_gather(fresh_v.astype(jnp.bfloat16), 'fs', axis=0, tiled=True)]
    ppermute x0 -> x7, starting transfers between devices: none -> 14.1 us  [the longest x3 9.02 us: collect(): lax.ppermute(going_down, axis, [(d, (d - 1) % ways) for d in range(ways)])]
    ppermute x0 -> x7, waiting for transfers between devices: none -> 11.9 us  [the longest x4 10.3 us: collect(): lax.ppermute(going_up, axis, [(d, (d + 1) % ways) for d in range(ways)])]
    dynamic_update_slice x0 -> x7, local copies, waits for them, and re-layouts: none -> 5.55 us  [the longest x4 3.56 us: collect(): lax.dynamic_update_slice_in_dim(full, going_up, (here - far) % ways * tur...]
    unnamed x32 -> x33, local copies, waits for them, and re-layouts: 11 us -> 9.01 us
  transfers between devices with their start and end apart: 3 -> 9, of which waited for: 3 -> 8; matrix products, arithmetic and copies ran while one was open for 3% -> 7% of each run, Pallas kernels for 0% -> 0%
where the time goes in v1:
time: 188 us; the launch traced here: 187 us
  waiting for transfers between devices  88.2 us (47%)
  blocking collectives  39.8 us (21%)
  local copies, waits for them, and re-layouts  17.4 us (9%)
  between operations  15.6 us (8%)
  starting transfers between devices  14.2 us (8%)
  other arithmetic  5.96 us (3%)
  matrix products  5.85 us (3%)
    reduce_scatter x1, waiting for transfers between devices, per_device(): lax.psum_scatter(high + lax.dot_general(inputs, lower_part, contract, pre...  70.6 us
    psum x1, blocking collectives, per_device(): lax.psum((jnp.sum(direction_q * direction_q), jnp.sum(direction_v * direc...  39.8 us
    ppermute x4, waiting for transfers between devices, collect(): lax.ppermute(going_up, axis, [(d, (d + 1) % ways) for d in range(ways)])  10.3 us
    ppermute x3, starting transfers between devices, collect(): lax.ppermute(going_down, axis, [(d, (d - 1) % ways) for d in range(ways)])  9.02 us
    unnamed x33, local copies, waits for them, and re-layouts  9.01 us
    all_gather x1, waiting for transfers between devices, per_device(): lax.all_gather(fresh_v.astype(jnp.bfloat16), 'fs', axis=0, tiled=True)  5.64 us
    ppermute x4, starting transfers between devices, collect(): lax.ppermute(going_up, axis, [(d, (d + 1) % ways) for d in range(ways)])  5.09 us
  transfers between devices with their start and end apart: 9, of which 8 were waited for; matrix products, arithmetic and copies ran while one was open for 7% of the time, Pallas kernels for 0%

profile of v1, /device:TPU:0, one launch (start us, length us, event | category | flops | bytes accessed | tf_op | source)
XLA Modules:
  0.0 187.0 jit_solution(2433859172806822182)
XLA Ops:
  7.2 0.0 copy-start
  7.2 0.0 reduce-scatter.2.cloned.1.call-start
  7.2 1.0 reshape.52
  8.2 0.0 copy-start.4
  8.2 0.8 reshape.55
  9.0 0.0 copy-start.5
  9.0 1.2 copy.40
  10.2 1.2 copy.42
  11.4 0.2 fusion.10
  11.6 0.2 fusion.7
  11.8 1.0 fusion.2
  12.8 0.0 copy-start.6
  12.8 2.3 %fusion = f32[2048,256]{0,1:T(8,128)} fusion(f32[256,2048]{1,0:T(8,128)S(1)} %fusion.2, bf16[576,2048]{1,0:T(8,128)(2,1)S(1)} %copy-done, f32[576,128]{0,1:T(8,128)S(1)} %bitcast.31, f32[576,128]{0,1:T(8,128)S(1)} %bitcast.29), kind=kOutput, calls=%fused_computation.1 | convolution fusion | flops 605241344 | bytes 7143424 | tf_op jit(solution)/shard_map/dot_general | solution.py:83
  15.1 0.0 copy-done.5
  15.2 0.0 copy-start.9
  15.2 0.0 reduce-scatter.2.cloned.1.call-update
  15.2 0.0 all-gather.2.cloned.1.call-start
  15.2 0.1 copy.39
  15.4 0.7 copy-done.7
  16.0 0.1 copy.44
  16.2 0.1 copy.46
  16.3 0.1 copy.47
  16.4 70.6 %reduce-scatter.2.cloned.1.call-done = f32[256,256]{0,1:T(8,128)} async-done(((f32[2048,256]{0,1:T(8,128)}), f32[256,256]{0,1:T(8,128)}) %reduce-scatter.2.cloned.1.call-update) | async-done | bytes 262160 | tf_op jit(solution)/shard_map/reduce_scatter | solution.py:82
  86.9 2.4 %multiply_reduce_fusion = (f32[]{:T(128)}, f32[256,128]{0,1:T(8,128)S(1)}, f32[256,128]{0,1:T(8,128)}, f32[256,128]{0,1:T(8,128)S(1)}, f32[]{:T(128)}, /*index=5...) fusion(f32[256,256]{0,1:T(8,128)} %reduce-scatter.2.cloned.1.call-done, f32[256,128]{0,1:T(8,128)S(1)} %copy.47, ...), kind=kLoop, calls=%fused_computation.14 | loop fusion | flops 720894 | bytes 1572872 | tf_op jit(solution)/shard_map/reduce_sum | solution.py:93
  89.3 39.8 %all-reduce = (f32[]{:T(128)}, f32[]{:T(128)}) all-reduce(f32[]{:T(128)} %get-tuple-element.45, f32[]{:T(128)} %get-tuple-element.37), channel_id=1, replica_groups=mesh['fs'=8,'tp'=4] {'fs','tp'}, use_global_device_ids=true, to_apply=%region_2.0 | all-reduce | flops 2 | bytes 16 | tf_op jit(solution)/shard_map/psum | solution.py:92
  129.8 1.1 convolution_multiply_fusion
  130.9 0.1 copy.52
  131.0 0.0 copy-start.1
  131.0 1.8 fusion.14
  132.8 0.0 all-gather.2.cloned.1.call-update
  133.6 1.1 convolution_multiply_fusion.1
  134.6 0.1 copy.51
  134.8 0.0 copy-start.2
  134.8 0.0 copy-start.3
  134.8 1.0 broadcast_in_dim.3
  135.8 1.8 constant_dynamic-update-slice_fusion.7
  137.6 2.5 %collective-permute-start = (bf16[256,256]{1,0:T(8,128)(2,1)}, bf16[256,256]{1,0:T(8,128)(2,1)}, u32[]{:S(2)}, u32[]{:S(2)}) collective-permute-start(bf16[256,256]{1,0:T(8,128)(2,1)} %get-tuple-element.35), channel_id=1, source_target_pairs={{0,4},{4,8},{8,12},{12,16},{16,20},{20,24},{24,28},{28,0},{1,5},{5... | collective-permute-start | bytes 393224 | tf_op jit(solution)/shard_map/ppermute | solution.py:18
  140.1 2.3 %collective-permute-start.1 = (bf16[256,256]{1,0:T(8,128)(2,1)}, bf16[256,256]{1,0:T(8,128)(2,1)S(1)}, u32[]{:S(2)}, u32[]{:S(2)}) collective-permute-start(bf16[256,256]{1,0:T(8,128)(2,1)} %get-tuple-element.35), channel_id=1, source_target_pairs={{0,28},{4,0},{8,4},{12,8},{16,12},{20,16},{24,20},{28,24},{1,29},{... | collective-permute-start | bytes 393224 | tf_op jit(solution)/shard_map/ppermute | solution.py:21
  142.3 0.8 copy.56
  143.1 0.8 copy.55
  143.8 0.0 copy-done.1
  143.8 0.8 copy.54
  144.6 0.8 copy.53
  145.4 0.5 collective-permute-done
  145.8 2.6 %collective-permute-start.2 = (bf16[256,256]{1,0:T(8,128)(2,1)}, bf16[256,256]{1,0:T(8,128)(2,1)S(1)}, u32[]{:S(2)}, u32[]{:S(2)}) collective-permute-start(bf16[256,256]{1,0:T(8,128)(2,1)} %collective-permute-done), channel_id=1, source_target_pairs={{0,4},{4,8},{8,12},{12,16},{16,20},{20,24},{24,28},{28,0},{1,5},{5... | collective-permute-start | bytes 393224 | tf_op jit(solution)/shard_map/ppermute | solution.py:18
  148.5 0.1 collective-permute-done.1
  148.6 2.0 %collective-permute-start.3 = (bf16[256,256]{1,0:T(8,128)(2,1)S(1)}, bf16[256,256]{1,0:T(8,128)(2,1)S(1)}, u32[]{:S(2)}, u32[]{:S(2)}) collective-permute-start(bf16[256,256]{1,0:T(8,128)(2,1)S(1)} %collective-permute-done.1), channel_id=1, source_target_pairs={{0,28},{4,0},{8,4},{12,8},{16,12},{20,16},{24,20},{28,24},{1,29},{... | collective-permute-start | bytes 393224 | tf_op jit(solution)/shard_map/ppermute | solution.py:21
  150.6 1.6 constant_dynamic-update-slice_fusion.6
  152.2 0.7 constant_dynamic-update-slice_fusion.5
  152.9 2.8 %collective-permute-done.2 = bf16[256,256]{1,0:T(8,128)(2,1)S(1)} collective-permute-done((bf16[256,256]{1,0:T(8,128)(2,1)}, bf16[256,256]{1,0:T(8,128)(2,1)S(1)}, u32[]{:S(2)}, u32[]{:S(2)}) %collective-permute-start.2) | collective-permute-done | bytes 131104 | tf_op jit(solution)/shard_map/ppermute | solution.py:18
  155.7 0.0 collective-permute-start.4
  155.7 0.0 collective-permute-done.3
  155.7 4.7 %collective-permute-start.5 = (bf16[256,256]{1,0:T(8,128)(2,1)S(1)}, bf16[256,256]{1,0:T(8,128)(2,1)S(1)}, u32[]{:S(2)}, u32[]{:S(2)}) collective-permute-start(bf16[256,256]{1,0:T(8,128)(2,1)S(1)} %collective-permute-done.3), channel_id=1, source_target_pairs={{0,28},{4,0},{8,4},{12,8},{16,12},{20,16},{24,20},{28,24},{1,29},{... | collective-permute-start | bytes 393224 | tf_op jit(solution)/shard_map/ppermute | solution.py:21
  160.4 0.7 constant_dynamic-update-slice_fusion.4
  161.1 0.7 constant_dynamic-update-slice_fusion.3
  161.7 1.6 collective-permute-done.4
  163.4 0.0 collective-permute-start.6
  163.4 0.7 constant_dynamic-update-slice_fusion.2
  164.0 1.5 collective-permute-done.5
  165.5 0.7 constant_dynamic-update-slice_fusion.1
  166.2 5.4 %collective-permute-done.6 = bf16[256,256]{1,0:T(8,128)(2,1)S(1)} collective-permute-done((bf16[256,256]{1,0:T(8,128)(2,1)S(1)}, bf16[256,256]{1,0:T(8,128)(2,1)S(1)}, u32[]{:S(2)}, u32[]{:S(2)}) %collective-permute-start.6) | collective-permute-done | bytes 131104 | tf_op jit(solution)/shard_map/ppermute | solution.py:18
  171.6 0.7 constant_dynamic-update-slice_fusion
  172.2 5.6 %all-gather.2.cloned.1.call-done = bf16[2048,256]{1,0:T(8,128)(2,1)} async-done(((bf16[256,256]{1,0:T(8,128)(2,1)}), bf16[2048,256]{1,0:T(8,128)(2,1)}) %all-gather.2.cloned.1.call-update) | async-done | bytes 1048592 | tf_op jit(solution)/shard_map/all_gather | solution.py:104
  177.9 2.3 %copy.74 = bf16[2048,256]{1,0:T(8,128)(2,1)} copy(bf16[2048,256]{1,0:T(8,128)(2,1)} %all-gather.2.cloned.1.call-done) | data formatting | bytes 2097152
  (9 shorter events, 0.0 us)
Async XLA Ops:
  7.2 4.6 %copy-start = (bf16[576,2048]{1,0:T(8,128)(2,1)S(1)}, bf16[576,2048]{1,0:T(8,128)(2,1)}, u32[]{:S(2)}) copy-start(bf16[576,2048]{1,0:T(8,128)(2,1)} %param.11) | copy-start | bytes 7077892
  7.2 79.7 %reduce-scatter.2.cloned.1.call-start = ((), (), s32[]{:S(2)}) async-start(), calls=%async_computation.1 | async-start | bytes 2359296 | tf_op jit(solution)/shard_map/reduce_scatter | solution.py:82
  8.2 6.9 %copy-start.4 = (bf16[4,64,32]{1,0,2:T(4,128)(2,1)}, bf16[4,64,32]{1,0,2:T(4,128)(2,1)S(1)}, u32[]{:S(2)}) copy-start(bf16[4,64,32]{1,0,2:T(4,128)(2,1)S(1)} %reshape.52) | copy-start | bytes 49156
  9.0 6.1 %copy-start.5 = (bf16[4,64,32]{1,0,2:T(4,128)(2,1)}, bf16[4,64,32]{1,0,2:T(4,128)(2,1)S(1)}, u32[]{:S(2)}) copy-start(bf16[4,64,32]{1,0,2:T(4,128)(2,1)S(1)} %reshape.55) | copy-start | bytes 49156
  12.8 2.5 %copy-start.6 = (f32[256,128]{1,0:T(8,128)S(1)}, f32[256,128]{1,0:T(8,128)}, u32[]{:S(2)}) copy-start(f32[256,128]{1,0:T(8,128)} %param.18) | copy-start | bytes 393220
  15.1 0.9 copy-start.7
  15.1 1.0 copy-start.8
  15.2 1.1 copy-start.9
  15.2 162.7 %all-gather.2.cloned.1.call-start = ((), (), s32[]{:S(2)}) async-start(), calls=%async_computation.2 | async-start | bytes 1179648 | tf_op jit(solution)/shard_map/all_gather | solution.py:104
  131.0 12.8 %copy-start.1 = (f32[256,256]{1,0:T(8,128)}, f32[256,256]{1,0:T(8,128)S(1)}, u32[]{:S(2)}) copy-start(f32[256,256]{1,0:T(8,128)S(1)} %copy.52) | copy-start | bytes 786436
  134.8 31.4 %copy-start.2 = (f32[256,256]{1,0:T(8,128)}, f32[256,256]{1,0:T(8,128)S(1)}, u32[]{:S(2)}) copy-start(f32[256,256]{1,0:T(8,128)S(1)} %copy.51) | copy-start | bytes 786436
  134.8 7.6 %copy-start.3 = (f32[256,128]{0,1:T(8,128)S(1)}, f32[256,128]{0,1:T(8,128)}, u32[]{:S(2)}) copy-start(f32[256,128]{0,1:T(8,128)} %get-tuple-element.39) | copy-start | bytes 393220
  137.6 8.2 %collective-permute-start = (bf16[256,256]{1,0:T(8,128)(2,1)}, bf16[256,256]{1,0:T(8,128)(2,1)}, u32[]{:S(2)}, u32[]{:S(2)}) collective-permute-start(bf16[256,256]{1,0:T(8,128)(2,1)} %get-tuple-element.35), channel_id=1, source_target_pairs={{0,4},{4,8},{8,12},{12,16},{16,20},{20,24},{24,28},{28,0},{1,5},{5... | collective-permute-start | bytes 393224 | tf_op jit(solution)/shard_map/ppermute | solution.py:18
  140.1 8.5 %collective-permute-start.1 = (bf16[256,256]{1,0:T(8,128)(2,1)}, bf16[256,256]{1,0:T(8,128)(2,1)S(1)}, u32[]{:S(2)}, u32[]{:S(2)}) collective-permute-start(bf16[256,256]{1,0:T(8,128)(2,1)} %get-tuple-element.35), channel_id=1, source_target_pairs={{0,28},{4,0},{8,4},{12,8},{16,12},{20,16},{24,20},{28,24},{1,29},{... | collective-permute-start | bytes 393224 | tf_op jit(solution)/shard_map/ppermute | solution.py:21
  145.8 9.8 %collective-permute-start.2 = (bf16[256,256]{1,0:T(8,128)(2,1)}, bf16[256,256]{1,0:T(8,128)(2,1)S(1)}, u32[]{:S(2)}, u32[]{:S(2)}) collective-permute-start(bf16[256,256]{1,0:T(8,128)(2,1)} %collective-permute-done), channel_id=1, source_target_pairs={{0,4},{4,8},{8,12},{12,16},{16,20},{20,24},{24,28},{28,0},{1,5},{5... | collective-permute-start | bytes 393224 | tf_op jit(solution)/shard_map/ppermute | solution.py:18
  148.6 7.1 %collective-permute-start.3 = (bf16[256,256]{1,0:T(8,128)(2,1)S(1)}, bf16[256,256]{1,0:T(8,128)(2,1)S(1)}, u32[]{:S(2)}, u32[]{:S(2)}) collective-permute-start(bf16[256,256]{1,0:T(8,128)(2,1)S(1)} %collective-permute-done.1), channel_id=1, source_target_pairs={{0,28},{4,0},{8,4},{12,8},{16,12},{20,16},{24,20},{28,24},{1,29},{... | collective-permute-start | bytes 393224 | tf_op jit(solution)/shard_map/ppermute | solution.py:21
  155.7 7.7 %collective-permute-start.4 = (bf16[256,256]{1,0:T(8,128)(2,1)S(1)}, bf16[256,256]{1,0:T(8,128)(2,1)S(1)}, u32[]{:S(2)}, u32[]{:S(2)}) collective-permute-start(bf16[256,256]{1,0:T(8,128)(2,1)S(1)} %collective-permute-done.2), channel_id=1, source_target_pairs={{0,4},{4,8},{8,12},{12,16},{16,20},{20,24},{24,28},{28,0},{1,5},{5... | collective-permute-start | bytes 393224 | tf_op jit(solution)/shard_map/ppermute | solution.py:18
  155.7 9.8 %collective-permute-start.5 = (bf16[256,256]{1,0:T(8,128)(2,1)S(1)}, bf16[256,256]{1,0:T(8,128)(2,1)S(1)}, u32[]{:S(2)}, u32[]{:S(2)}) collective-permute-start(bf16[256,256]{1,0:T(8,128)(2,1)S(1)} %collective-permute-done.3), channel_id=1, source_target_pairs={{0,28},{4,0},{8,4},{12,8},{16,12},{20,16},{24,20},{28,24},{1,29},{... | collective-permute-start | bytes 393224 | tf_op jit(solution)/shard_map/ppermute | solution.py:21
  163.4 8.2 %collective-permute-start.6 = (bf16[256,256]{1,0:T(8,128)(2,1)S(1)}, bf16[256,256]{1,0:T(8,128)(2,1)S(1)}, u32[]{:S(2)}, u32[]{:S(2)}) collective-permute-start(bf16[256,256]{1,0:T(8,128)(2,1)S(1)} %collective-permute-done.4), channel_id=1, source_target_pairs={{0,4},{4,8},{8,12},{12,16},{16,20},{20,24},{24,28},{28,0},{1,5},{5... | collective-permute-start | bytes 393224 | tf_op jit(solution)/shard_map/ppermute | solution.py:18
Sparse Core Ops, SparseCore 0:
  15.3 71.5 reduce-scatter.1
  133.0 44.8 all-gather.1
